TPU v7x, 32 devices: a whole 2x2x4 slice. The times are simulated.
32 devices in a mesh: ep: 4 (over y, x), tp: 8 (over z, core).
Axes of the slice: x: 2, y: 2, z: 4, core: 2. Of those that a mesh axis runs over, the one named last changes fastest.
Arguments:
- queries: bfloat16 [4096, 1024], P('ep', 'tp'), may hold values from -6 to 6
- keys: bfloat16 [4096, 256], P('ep'), may hold values from -6 to 6, as said below
- values: bfloat16 [4096, 256], P('ep'), may hold values from -6 to 6
- slopes: float32 [16], P('tp'), may hold values from 0.002 to 0.08
- sinks: float32 [16], P('tp'), may hold values from 2 to 6
- out_weight: bfloat16 [1024, 2048], P('tp'), may hold values from -0.1875 to 0.1875
- mix_gain: float32 [2048], replicated, may hold values from 0.1 to 1.9
- moe_input: bfloat16 [4096, 2048], P(('ep', 'tp')), may hold values from -6 to 6
- in_gain: float32 [2048], replicated, may hold values from 0.1 to 1.9
- out_gain: float32 [2048], replicated, may hold values from 0.1 to 1.9
- group_router: bfloat16 [2048, 4], replicated, may hold values from -0.125 to 0.125
- expert_router: bfloat16 [2048, 4], replicated, may hold values from -0.125 to 0.125
- routes: int32 [4096, 2], P(('ep', 'tp')), may hold values from 0 to 3, all different within a row; in each aligned block of 128 rows (0 to 127, 128 to 255, ...) at most 96 rows name the same one
- gate_weight: bfloat16 [4, 2048, 1024], P('ep', None, 'tp'), may hold values from -0.125 to 0.125
- up_weight: bfloat16 [4, 2048, 1024], P('ep', None, 'tp'), may hold values from -0.125 to 0.125
- down_weight: bfloat16 [4, 2048, 1024], P('ep', None, 'tp'), may hold values from -0.1875 to 0.1875
Outputs:
- mixer_output: bfloat16 [4096, 2048], P(('ep', 'tp'))
- moe_output: bfloat16 [4096, 2048], P(('ep', 'tp'))
Inputs may be any that keep to these rules, and one draw needn't show every extreme that they name: `keys`: keys share one value range with the queries. `routes`: A token names 2 different experts. Among the rows of one device no expert is named more than 96 times, a bound that some block reaches in every draw.
All inputs are finite; a program needn't handle non-finite values.
Results may differ from a plain program's by a relative error of at most 0.018.
Values may be sent and summed in bfloat16 or wider, within the bound.
No kernel may reach another device: no remote copies, remote signals or barrier semaphores. Data moves between devices by JAX's collectives and lax.ppermute only.
A program may use at most 128 MiB of HBM per device.

v0:
```python
import math
import jax
import jax.numpy as jnp
from jax import lax
from jax.sharding import PartitionSpec as P

HEADS = 16
HD = 64
KV_HEADS = 4
WINDOW = 128
eps = 1e-06


def shifted(block, axis, distance):
    devices = range(lax.axis_size(axis))
    route = [(i - distance, i) for i in devices if i - distance in devices]
    return lax.ppermute(block, axis, route)


def scale_rows(matrix, gain):
    mean_square = jnp.mean(matrix * matrix, axis=-1, keepdims=True)
    return matrix * lax.rsqrt(mean_square + eps) * gain


def per_device(
    queries,
    keys,
    values,
    slopes,
    sinks,
    out_weight,
    mix_gain,
    moe_input,
    in_gain,
    out_gain,
    group_router,
    expert_router,
    routes,
    gate_weight,
    up_weight,
    down_weight,
):
    rows_group = queries.shape[0]
    local_heads = slopes.shape[0]
    per_kv = HEADS // KV_HEADS
    kv_index = lax.axis_index("tp") * local_heads // per_kv
    own_keys = lax.dynamic_slice_in_dim(keys, kv_index * HD, HD, 1)
    own_values = lax.dynamic_slice_in_dim(values, kv_index * HD, HD, 1)
    rim_keys, rim_values = shifted(
        (own_keys[rows_group - WINDOW :], own_values[rows_group - WINDOW :]), "ep", 1
    )
    blocks = rows_group // WINDOW
    key_blocks = own_keys.reshape(blocks, WINDOW, HD)
    value_blocks = own_values.reshape(blocks, WINDOW, HD)
    key_span = jnp.concatenate(
        [jnp.concatenate([rim_keys[None], key_blocks[:-1]], axis=0), key_blocks], axis=1
    )
    value_span = jnp.concatenate(
        [jnp.concatenate([rim_values[None], value_blocks[:-1]], axis=0), value_blocks], axis=1
    )
    query_blocks = queries.reshape(blocks, WINDOW, local_heads, HD)
    scores = jnp.einsum(
        "nqhd,nsd->nhqs", query_blocks, key_span, preferred_element_type=jnp.float32
    ) * (1.0 / math.sqrt(HD))
    query_index = jnp.arange(WINDOW, dtype=jnp.int32)[:, None]
    key_index = jnp.arange(2 * WINDOW, dtype=jnp.int32)[None, :]
    distance = query_index + WINDOW - key_index
    key_position = (
        lax.axis_index("ep") * rows_group
        + jnp.arange(blocks, dtype=jnp.int32)[:, None, None] * WINDOW
        + key_index[None]
        - WINDOW
    )
    valid = ((distance >= 0) & (distance < WINDOW))[None] & (key_position >= 0)
    scores = scores - slopes[None, :, None, None] * distance.astype(jnp.float32)[None, None]
    scores = jnp.where(valid[:, None], scores, -jnp.inf)
    sink = sinks[None, :, None, None]
    top = jnp.maximum(jnp.max(scores, axis=-1, keepdims=True), sink)
    weights = jnp.exp(scores - top)
    denom = jnp.sum(weights, axis=-1, keepdims=True) + jnp.exp(sink - top)
    probs = (weights / denom).astype(jnp.bfloat16)
    attention = jnp.einsum("nhqs,nsd->nqhd", probs, value_span, preferred_element_type=jnp.float32)
    attention = attention.astype(jnp.bfloat16).reshape(rows_group, local_heads * HD)
    own_rows = moe_input.shape[0]
    projected = lax.psum_scatter(
        jnp.dot(attention, out_weight, preferred_element_type=jnp.float32).astype(jnp.bfloat16),
        "tp",
        scatter_dimension=0,
        tiled=True,
    ).astype(jnp.float32)
    mixer_output = scale_rows(projected, mix_gain).astype(jnp.bfloat16)
    normed = scale_rows(moe_input.astype(jnp.float32), in_gain).astype(jnp.bfloat16)
    group_logits = jnp.dot(normed, group_router, preferred_element_type=jnp.float32)
    expert_logits = jnp.dot(normed, expert_router, preferred_element_type=jnp.float32)
    experts = expert_router.shape[1]
    groups = group_router.shape[1]
    per_group = experts // groups
    visits = routes.shape[1]
    expert_match = routes[:, :, None] == jnp.arange(experts, dtype=jnp.int32)[None, None, :]
    picked_logits = jnp.sum(jnp.where(expert_match, expert_logits[:, None, :], 0.0), axis=-1)
    group_prob = jax.nn.softmax(group_logits, axis=-1)
    group_match = (routes // per_group)[:, :, None] == jnp.arange(groups, dtype=jnp.int32)[
        None, None, :
    ]
    picked_group = jnp.sum(jnp.where(group_match, group_prob[:, None, :], 0.0), axis=-1)
    route_weight = picked_group * jax.nn.softmax(picked_logits, axis=-1)
    capacity = max(2, 3 * own_rows * visits // (2 * experts))
    match_int = expert_match.astype(jnp.int32).reshape(own_rows * visits, experts)
    before = jnp.cumsum(match_int, axis=0) - match_int
    slot = jnp.sum(before * match_int, axis=-1)
    position = (routes.reshape(-1) * capacity + slot).reshape(own_rows, visits)
    slot_ids = jnp.arange(experts * capacity, dtype=jnp.int32)
    placement = jnp.any(position[None, :, :] == slot_ids[:, None, None], axis=-1).astype(
        jnp.bfloat16
    )
    outgoing = jnp.dot(placement, normed, preferred_element_type=jnp.float32).astype(jnp.bfloat16)
    local_experts = gate_weight.shape[0]
    outgoing = outgoing.reshape(lax.axis_size("ep"), local_experts, capacity, normed.shape[1])
    arrived = lax.all_to_all(outgoing, "ep", split_axis=0, concat_axis=0, tiled=True)
    gate_piece = lax.all_gather(gate_weight, "tp", axis=2, tiled=True)
    up_piece = lax.all_gather(up_weight, "tp", axis=2, tiled=True)
    down_piece = lax.all_gather(down_weight, "tp", axis=2, tiled=True)
    gate = jnp.einsum("sxcd,xdf->sxcf", arrived, gate_piece, preferred_element_type=jnp.float32)
    up = jnp.einsum("sxcd,xdf->sxcf", arrived, up_piece, preferred_element_type=jnp.float32)
    hidden = (jax.nn.silu(gate) * up).astype(jnp.bfloat16)
    results = jnp.einsum("sxcf,xdf->sxcd", hidden, down_piece, preferred_element_type=jnp.float32)
    returned = lax.all_to_all(
        results.astype(jnp.bfloat16), "ep", split_axis=0, concat_axis=0, tiled=True
    )
    flat_back = returned.reshape(experts * capacity, returned.shape[3])
    picked_rows = jnp.take(flat_back, position.reshape(-1), axis=0).reshape(
        own_rows, visits, flat_back.shape[1]
    )
    moe = jnp.sum(route_weight[:, :, None] * picked_rows.astype(jnp.float32), axis=1)
    moe_output = scale_rows(moe, out_gain).astype(jnp.bfloat16)
    return (mixer_output, moe_output)


def solution(mesh):
    return jax.shard_map(
        per_device,
        mesh=mesh,
        in_specs=(
            P("ep", "tp"),
            P("ep", None),
            P("ep", None),
            P("tp"),
            P("tp"),
            P("tp", None),
            P(),
            P(("ep", "tp"), None),
            P(),
            P(),
            P(),
            P(),
            P(("ep", "tp"), None),
            P("ep", None, "tp"),
            P("ep", None, "tp"),
            P("ep", None, "tp"),
        ),
        out_specs=(P(("ep", "tp"), None), P(("ep", "tp"), None)),
        check_vma=False,
    )
```

profile of v0, /device:TPU:0, one launch (start us, length us, event | category | flops | bytes accessed | tf_op | source)
XLA Modules:
  0.0 222.8 jit_solution(3067624268574023449)
XLA Ops:
  7.2 0.7 all-gather.6.cloned.1.call-update
  8.0 0.7 all-gather.4.cloned.1.call-update
  8.7 0.7 all-gather.8.cloned.1.call-update
  9.5 1.2 constant_dynamic-slice_fusion
  10.7 0.1 copy.112
  10.9 4.9 %collective-permute-start.1 = (bf16[128,64]{0,1:T(8,128)(2,1)S(1)}, bf16[128,64]{0,1:T(8,128)(2,1)S(1)}, u32[]{:S(2)}, u32[]{:S(2)}) collective-permute-start(bf16[128,64]{0,1:T(8,128)(2,1)S(1)} %slice.36), channel_id=1, source_target_pairs={{0,8},{8,16},{16,24},{1,9},{9,17},{17,25},{2,10},{10,18},{18,26},{... | collective-permute-start | bytes 49160 | tf_op jit(solution)/shard_map/ppermute | solution.py:17
  15.8 0.1 copy.111
  15.9 3.4 %collective-permute-start = (bf16[128,64]{0,1:T(8,128)(2,1)S(1)}, bf16[128,64]{0,1:T(8,128)(2,1)S(1)}, u32[]{:S(2)}, u32[]{:S(2)}) collective-permute-start(bf16[128,64]{0,1:T(8,128)(2,1)S(1)} %slice.34), channel_id=1, source_target_pairs={{0,8},{8,16},{16,24},{1,9},{9,17},{17,25},{2,10},{10,18},{18,26},{... | collective-permute-start | bytes 49160 | tf_op jit(solution)/shard_map/ppermute | solution.py:17
  19.6 0.3 broadcast_and_fusion
  19.9 0.1 broadcast_multiply_fusion
  20.1 0.2 reshape.313
  20.3 0.6 fusion.73
  21.1 0.3 fusion.13
  21.5 0.5 fusion.20
  22.0 0.2 copy.95
  22.2 3.2 %convolution_convert_fusion = bf16[1024,2048]{1,0:T(8,128)(2,1)} fusion(bf16[128,2048]{1,0:T(8,128)(2,1)S(1)} %copy-done, bf16[16,8,8,128]{3,2,1,0:T(8,128)(2,1)S(1)} %bitcast.155), kind=kOutput, calls=%fused_computation.7 | convolution fusion | flops 538968064 | bytes 4980736 | tf_op jit(solution)/shard_map/dot_general | solution.py:86
  25.4 0.6 copy-done.3
  26.1 0.1 copy.97
  26.2 0.1 eq.56
  26.3 0.1 reshape.291
  26.5 1.2 reduce-window.6
  27.8 0.1 copy.99
  27.9 0.1 copy.100
  28.1 0.1 reduce_sum.102
  28.4 0.2 fusion.33
  28.6 1.8 convolution_convert_fusion.1
  30.4 3.9 %all-to-all-start = ((bf16[4,1,96,2048]{3,2,1,0:T(8,128)(2,1)}), bf16[4,1,96,2048]{3,2,1,0:T(8,128)(2,1)S(1)}, u32[]{:S(2)}, u32[]{:S(2)}) async-start(bf16[4,1,96,2048]{3,2,1,0:T(8,128)(2,1)} %bitcast.11), calls=%async_computation.1 | async-start | bytes 3145728 | tf_op jit(solution)/shard_map/all_to_all | solution.py:119
  34.3 0.3 fusion.74
  34.7 0.3 fusion.68
  35.1 0.1 copy.96
  35.2 0.1 copy.105
  35.3 0.1 mul.175
  35.5 17.6 %all-to-all-done = bf16[4,1,96,2048]{3,2,1,0:T(8,128)(2,1)S(1)} async-done(((bf16[4,1,96,2048]{3,2,1,0:T(8,128)(2,1)}), bf16[4,1,96,2048]{3,2,1,0:T(8,128)(2,1)S(1)}, u32[]{:S(2)}, u32[]{:S(2)}) %all-to-all-start) | async-done | bytes 1572896 | tf_op jit(solution)/shard_map/all_to_all | solution.py:119
  53.1 7.1 %all-gather.6.cloned.1.call-done = bf16[1,2048,1024]{2,1,0:T(8,128)(2,1)} async-done(((bf16[1,2048,128]{2,1,0:T(8,128)(2,1)}), bf16[1,2048,1024]{2,1,0:T(8,128)(2,1)}) %all-gather.6.cloned.1.call-update) | async-done | bytes 4194320 | tf_op jit(solution)/shard_map/all_gather | solution.py:121
  60.2 5.1 %fusion.2 = f32[4,96,1024]{2,1,0:T(8,128)} fusion(bf16[1,2048,1024]{2,1,0:T(8,128)(2,1)} %all-gather.6.cloned.1.call-done, bf16[4,1,96,2048]{3,2,1,0:T(8,128)(2,1)S(1)} %all-to-all-done), kind=kOutput, calls=%fused_computation.3 | convolution fusion | flops 1610612736 | bytes 7340032 | tf_op jit(solution)/shard_map/sxcd,xdf->sxcf/dot_general | solution.py:124
  65.3 42.5 %all-gather.4.cloned.1.call-done = bf16[1,2048,1024]{2,1,0:T(8,128)(2,1)} async-done(((bf16[1,2048,128]{2,1,0:T(8,128)(2,1)}), bf16[1,2048,1024]{2,1,0:T(8,128)(2,1)}) %all-gather.4.cloned.1.call-update) | async-done | bytes 4194320 | tf_op jit(solution)/shard_map/all_gather | solution.py:120
  107.8 47.6 %all-gather.8.cloned.1.call-done = bf16[1,2048,1024]{2,1,0:T(8,128)(2,1)} async-done(((bf16[1,2048,128]{2,1,0:T(8,128)(2,1)}), bf16[1,2048,1024]{2,1,0:T(8,128)(2,1)}) %all-gather.8.cloned.1.call-update) | async-done | bytes 4194320 | tf_op jit(solution)/shard_map/all_gather | solution.py:122
  155.4 8.6 %fusion.9 = bf16[4,1,96,2048]{3,2,1,0:T(8,128)(2,1)} fusion(bf16[1,2048,1024]{2,1,0:T(8,128)(2,1)} %all-gather.8.cloned.1.call-done, f32[4,96,1024]{2,1,0:T(8,128)} %fusion.2, bf16[1,2048,1024]{2,1,0:T(8,128)(2,1)} %all-gather.4.cloned.1.call-done, bf16[4,1,96,2048]{3,2,1,0:T(8,128)(2,1)S(1)} %all-to-all-done), kind=kOutput, calls=%fused_computation.10 | convolution fusion | flops 3224371200 | bytes 13107200 | tf_op jit(solution)/shard_map/sxcf,xdf->sxcd/dot_general | solution.py:126
  164.1 3.9 %all-to-all-start.1 = ((bf16[4,1,96,2048]{3,2,1,0:T(8,128)(2,1)}), bf16[4,1,96,2048]{3,2,1,0:T(8,128)(2,1)S(1)}, u32[]{:S(2)}, u32[]{:S(2)}) async-start(bf16[4,1,96,2048]{3,2,1,0:T(8,128)(2,1)} %fusion.9), calls=%async_computation.2 | async-start | bytes 3145728 | tf_op jit(solution)/shard_map/all_to_all | solution.py:127
  167.9 0.1 copy.102
  168.1 37.6 %reduce-scatter.2.cloned.1.call-done = bf16[128,2048]{1,0:T(8,128)(2,1)} async-done(((bf16[1024,2048]{1,0:T(8,128)(2,1)}), bf16[128,2048]{1,0:T(8,128)(2,1)}) %reduce-scatter.2.cloned.1.call-update) | async-done | bytes 524304 | tf_op jit(solution)/shard_map/reduce_scatter | solution.py:85
  205.7 1.2 fusion.30
  207.0 2.0 fusion.32
  209.0 1.4 gather_fusion
  210.4 0.7 gather.7
  211.1 4.1 %multiply_reduce_fusion = f32[128,2048]{1,0:T(8,128)S(1)} fusion(bf16[128,2,2048]{2,1,0:T(2,128)(2,1)S(1)} %gather.7, pred[128,2]{1,0:T(8,128)(4,1)S(1)} %copy.102, f32[128,2]{1,0:T(8,128)S(1)} %copy.96), kind=kLoop, calls=%fused_computation.13 | loop fusion | flops 1835008 | bytes 2098432 | tf_op jit(solution)/shard_map/reduce_sum | solution.py:134
  215.2 0.2 multiply_reduce_fusion.1
  215.3 1.0 multiply_convert_fusion
  (63 shorter events, 1.2 us)
Async XLA Ops:
  7.2 15.0 %copy-start = (bf16[128,2048]{1,0:T(8,128)(2,1)S(1)}, bf16[128,2048]{1,0:T(8,128)(2,1)}, u32[]{:S(2)}) copy-start(bf16[128,2048]{1,0:T(8,128)(2,1)} %param.21) | copy-start | bytes 1572868
  7.2 53.0 %all-gather.6.cloned.1.call-start = ((), (), s32[]{:S(2)}) async-start(), calls=%async_computation.5 | async-start | bytes 4718592 | tf_op jit(solution)/shard_map/all_gather | solution.py:121
  7.9 12.0 %copy-start.8 = (f32[2]{0:T(128)S(1)}, f32[2]{0:T(128)}, u32[]{:S(2)}) copy-start(f32[2]{0:T(128)} %param.19) | copy-start | bytes 28
  7.9 99.9 %all-gather.4.cloned.1.call-start = ((), (), s32[]{:S(2)}) async-start(), calls=%async_computation.4 | async-start | bytes 4718592 | tf_op jit(solution)/shard_map/all_gather | solution.py:120
  8.7 11.4 %copy-start.2 = (bf16[1024,128]{1,0:T(8,128)(2,1)S(1)}, bf16[1024,128]{1,0:T(8,128)(2,1)}, u32[]{:S(2)}) copy-start(bf16[1024,128]{1,0:T(8,128)(2,1)} %param.16) | copy-start | bytes 786436
  8.7 146.7 %all-gather.8.cloned.1.call-start = ((), (), s32[]{:S(2)}) async-start(), calls=%async_computation.6 | async-start | bytes 4718592 | tf_op jit(solution)/shard_map/all_gather | solution.py:122
  9.4 196.3 %reduce-scatter.2.cloned.1.call-start = ((), (), s32[]{:S(2)}) async-start(), calls=%async_computation.3 | async-start | bytes 4718592 | tf_op jit(solution)/shard_map/reduce_scatter | solution.py:85
  10.9 9.4 %collective-permute-start.1 = (bf16[128,64]{0,1:T(8,128)(2,1)S(1)}, bf16[128,64]{0,1:T(8,128)(2,1)S(1)}, u32[]{:S(2)}, u32[]{:S(2)}) collective-permute-start(bf16[128,64]{0,1:T(8,128)(2,1)S(1)} %slice.36), channel_id=1, source_target_pairs={{0,8},{8,16},{16,24},{1,9},{9,17},{17,25},{2,10},{10,18},{18,26},{... | collective-permute-start | bytes 49160 | tf_op jit(solution)/shard_map/ppermute | solution.py:17
  15.9 5.6 %collective-permute-start = (bf16[128,64]{0,1:T(8,128)(2,1)S(1)}, bf16[128,64]{0,1:T(8,128)(2,1)S(1)}, u32[]{:S(2)}, u32[]{:S(2)}) collective-permute-start(bf16[128,64]{0,1:T(8,128)(2,1)S(1)} %slice.34), channel_id=1, source_target_pairs={{0,8},{8,16},{16,24},{1,9},{9,17},{17,25},{2,10},{10,18},{18,26},{... | collective-permute-start | bytes 49160 | tf_op jit(solution)/shard_map/ppermute | solution.py:17
  20.3 0.7 copy-start.7
  25.4 0.7 copy-start.3
  25.4 3.0 %copy-start.1 = (bf16[128,2048]{1,0:T(8,128)(2,1)S(1)}, bf16[128,2048]{1,0:T(8,128)(2,1)}, u32[]{:S(2)}) copy-start(bf16[128,2048]{1,0:T(8,128)(2,1)} %param.23) | copy-start | bytes 1572868
  25.4 3.2 %copy-start.4 = (f32[2048]{0:T(1024)S(1)}, f32[2048]{0:T(1024)}, u32[]{:S(2)}) copy-start(f32[2048]{0:T(1024)} %param.24) | copy-start | bytes 24580
  30.4 3.9 %copy-start.9 = (bf16[2048,4]{0,1:T(4,128)(2,1)S(1)}, bf16[2048,4]{0,1:T(4,128)(2,1)}, u32[]{:S(2)}) copy-start(bf16[2048,4]{0,1:T(4,128)(2,1)} %param.26) | copy-start | bytes 49156
  30.4 4.3 %copy-start.10 = (bf16[2048,4]{0,1:T(4,128)(2,1)S(1)}, bf16[2048,4]{0,1:T(4,128)(2,1)}, u32[]{:S(2)}) copy-start(bf16[2048,4]{0,1:T(4,128)(2,1)} %param.27) | copy-start | bytes 49156
  30.4 22.6 %all-to-all-start = ((bf16[4,1,96,2048]{3,2,1,0:T(8,128)(2,1)}), bf16[4,1,96,2048]{3,2,1,0:T(8,128)(2,1)S(1)}, u32[]{:S(2)}, u32[]{:S(2)}) async-start(bf16[4,1,96,2048]{3,2,1,0:T(8,128)(2,1)} %bitcast.11), calls=%async_computation.1 | async-start | bytes 3145728 | tf_op jit(solution)/shard_map/all_to_all | solution.py:119
  164.1 42.9 %copy-start.5 = (f32[2048]{0:T(1024)S(1)}, f32[2048]{0:T(1024)}, u32[]{:S(2)}) copy-start(f32[2048]{0:T(1024)} %param.22) | copy-start | bytes 24580
  164.1 44.9 %all-to-all-start.1 = ((bf16[4,1,96,2048]{3,2,1,0:T(8,128)(2,1)}), bf16[4,1,96,2048]{3,2,1,0:T(8,128)(2,1)S(1)}, u32[]{:S(2)}, u32[]{:S(2)}) async-start(bf16[4,1,96,2048]{3,2,1,0:T(8,128)(2,1)} %fusion.9), calls=%async_computation.2 | async-start | bytes 3145728 | tf_op jit(solution)/shard_map/all_to_all | solution.py:127
  211.1 4.3 %copy-start.6 = (f32[2048]{0:T(1024)S(1)}, f32[2048]{0:T(1024)}, u32[]{:S(2)}) copy-start(f32[2048]{0:T(1024)} %param.25) | copy-start | bytes 24580
Sparse Core Ops, SparseCore 0:
  9.6 50.5 all-gather.5
  61.7 45.9 all-gather.3
  109.4 45.9 all-gather.7
  157.6 48.1 reduce-scatter.1
where the time goes:
time: 223 us
  waiting for transfers between devices  155 us (70%)
  matrix products  20.5 us (9%)
  starting transfers between devices  16.2 us (7%)
  between operations  14.2 us (6%)
  other arithmetic  11.3 us (5%)
  local copies, waits for them, and re-layouts  6.18 us (3%)
    all_gather x1, waiting for transfers between devices, per_device(): down_piece = lax.all_gather(down_weight, 'tp', axis=2, tiled=True)  47.6 us
    all_gather x1, waiting for transfers between devices, per_device(): gate_piece = lax.all_gather(gate_weight, 'tp', axis=2, tiled=True)  42.5 us
    reduce_scatter x1, waiting for transfers between devices, per_device(): lax.psum_scatter(jnp.dot(attention, out_weight, preferred_element_type=jn...  37.6 us
    all_to_all x1, waiting for transfers between devices, per_device(): lax.all_to_all(outgoing, 'ep', split_axis=0, concat_axis=0, tiled=True)  17.6 us
    dot_general x1, matrix products, per_device(): jnp.einsum('sxcf,xdf->sxcd', hidden, down_piece, preferred_element_type=j...  8.63 us
    ppermute x2, starting transfers between devices, shifted(): return lax.ppermute(block, axis, route)  8.27 us
    all_gather x1, waiting for transfers between devices, per_device(): up_piece = lax.all_gather(up_weight, 'tp', axis=2, tiled=True)  7.09 us
    dot_general x1, matrix products, per_device(): jnp.einsum('sxcd,xdf->sxcf', arrived, up_piece, preferred_element_type=jn...  5.13 us
  transfers between devices with their start and end apart: 8, of which 5 were waited for; matrix products, arithmetic and copies ran while one was open for 13% of the time, Pallas kernels for 0%

commit v1 on v0

--- a/solution.py
+++ b/solution.py
@@ -3,6 +3,7 @@
 import jax.numpy as jnp
 from jax import lax
 from jax.sharding import PartitionSpec as P
+from jax.lax import axis_index, axis_size, ppermute
 
 HEADS = 16
 HD = 64
@@ -117,7 +118,19 @@
     local_experts = gate_weight.shape[0]
     outgoing = outgoing.reshape(lax.axis_size("ep"), local_experts, capacity, normed.shape[1])
     arrived = lax.all_to_all(outgoing, "ep", split_axis=0, concat_axis=0, tiled=True)
-    gate_piece = lax.all_gather(gate_weight, "tp", axis=2, tiled=True)
+    cores_n = axis_size("tp")
+    steps_seen = [(b, (b + 1) % cores_n) for b in range(cores_n)]
+    all_rows = [(b, (b - 1) % cores_n) for b in range(cores_n)]
+    piece_now, local_next = ([gate_weight], [gate_weight])
+    for _ in range(cores_n // 2):
+        piece_now.append(ppermute(piece_now[-1], "tp", steps_seen))
+    for _ in range((cores_n - 1) // 2):
+        local_next.append(ppermute(local_next[-1], "tp", all_rows))
+    gate_piece = jnp.roll(
+        jnp.concatenate([*piece_now[::-1], *local_next[1:]], 2),
+        (axis_index("tp") - cores_n // 2) * gate_weight.shape[2],
+        2,
+    )
     up_piece = lax.all_gather(up_weight, "tp", axis=2, tiled=True)
     down_piece = lax.all_gather(down_weight, "tp", axis=2, tiled=True)
     gate = jnp.einsum("sxcd,xdf->sxcf", arrived, gate_piece, preferred_element_type=jnp.float32)

time: 223 us -> 199 us (0.89)
  waiting for transfers between devices: 155 us -> 97.5 us
  local copies, waits for them, and re-layouts: 6.18 us -> 25.5 us
  starting transfers between devices: 16.2 us -> 29.4 us
    all_gather x1 -> x0, waiting for transfers between devices: 42.5 us -> none  [per_device(): gate_piece = lax.all_gather(gate_weight, 'tp', axis=2, tiled=True)]
    ppermute x0 -> x7, waiting for transfers between devices: none -> 33.8 us  [the longest x4 33.7 us: per_device(): piece_now.append(ppermute(piece_now[-1], 'tp', steps_seen))]
    all_gather x1, waiting for transfers between devices: 47.6 us -> 24.4 us  [per_device(): down_piece = lax.all_gather(down_weight, 'tp', axis=2, tiled=True)]
    unnamed x25 -> x42, local copies, waits for them, and re-layouts: 1.09 us -> 19.6 us
    all_to_all x1, waiting for transfers between devices: 17.6 us -> 0.01 us  [per_device(): lax.all_to_all(outgoing, 'ep', split_axis=0, concat_axis=0, tiled=True)]
    ppermute x0 -> x7, starting transfers between devices: none -> 13.8 us  [the longest x3 11.3 us: per_device(): local_next.append(ppermute(local_next[-1], 'tp', all_rows))]
    all_gather x1, waiting for transfers between devices: 7.09 us -> 0.01 us  [per_device(): up_piece = lax.all_gather(up_weight, 'tp', axis=2, tiled=True)]
  transfers between devices with their start and end apart: 8 -> 14, of which waited for: 5 -> 6; matrix products, arithmetic and copies ran while one was open for 13% -> 25% of each run, Pallas kernels for 0% -> 0%
where the time goes in v1:
time: 199 us; the launch traced here: 198 us
  waiting for transfers between devices  97.5 us (49%)
  starting transfers between devices  29.4 us (15%)
  local copies, waits for them, and re-layouts  25.5 us (13%)
  matrix products  20.1 us (10%)
  between operations  14.2 us (7%)
  other arithmetic  11.2 us (6%)
    reduce_scatter x1, waiting for transfers between devices, per_device(): lax.psum_scatter(jnp.dot(attention, out_weight, preferred_element_type=jn...  38 us
    ppermute x4, waiting for transfers between devices, per_device(): piece_now.append(ppermute(piece_now[-1], 'tp', steps_seen))  33.7 us
    all_gather x1, waiting for transfers between devices, per_device(): down_piece = lax.all_gather(down_weight, 'tp', axis=2, tiled=True)  24.4 us
    unnamed x42, local copies, waits for them, and re-layouts  19.6 us
    ppermute x3, starting transfers between devices, per_device(): local_next.append(ppermute(local_next[-1], 'tp', all_rows))  11.3 us
    dot_general x1, matrix products, per_device(): jnp.einsum('sxcf,xdf->sxcd', hidden, down_piece, preferred_element_type=j...  8.67 us
    ppermute x2, starting transfers between devices, shifted(): return lax.ppermute(block, axis, route)  7.23 us
    dot_general x1, matrix products, per_device(): jnp.einsum('sxcd,xdf->sxcf', arrived, up_piece, preferred_element_type=jn...  4.56 us
  transfers between devices with their start and end apart: 14, of which 6 were waited for; matrix products, arithmetic and copies ran while one was open for 25% of the time, Pallas kernels for 0%

profile of v1, /device:TPU:0, one launch (start us, length us, event | category | flops | bytes accessed | tf_op | source)
XLA Modules:
  0.0 197.9 jit_solution(2270993233735532060)
XLA Ops:
  7.2 0.7 all-gather.3.cloned.1.call-update
  8.0 0.7 all-gather.5.cloned.1.call-update
  8.7 0.5 collective-permute-start.2
  9.3 4.1 %collective-permute-start.6 = (bf16[1,2048,128]{2,1,0:T(8,128)(2,1)}, bf16[1,2048,128]{2,1,0:T(8,128)(2,1)S(1)}, u32[]{:S(2)}, u32[]{:S(2)}) collective-permute-start(bf16[1,2048,128]{2,1,0:T(8,128)(2,1)} %param.29), channel_id=1, source_target_pairs={{0,7},{1,0},{2,1},{3,2},{4,3},{5,4},{6,5},{7,6},{8,15},{9,8},{10,9... | collective-permute-start | bytes 1572872 | tf_op jit(solution)/shard_map/ppermute | solution.py:128
  13.4 1.2 constant_dynamic-slice_fusion
  14.8 3.8 %collective-permute-start.1 = (bf16[128,64]{0,1:T(8,128)(2,1)S(1)}, bf16[128,64]{0,1:T(8,128)(2,1)S(1)}, u32[]{:S(2)}, u32[]{:S(2)}) collective-permute-start(bf16[128,64]{0,1:T(8,128)(2,1)S(1)} %slice.36), channel_id=1, source_target_pairs={{0,8},{8,16},{16,24},{1,9},{9,17},{17,25},{2,10},{10,18},{18,26},{... | collective-permute-start | bytes 49160 | tf_op jit(solution)/shard_map/ppermute | solution.py:18
  18.8 3.4 %collective-permute-start = (bf16[128,64]{0,1:T(8,128)(2,1)S(1)}, bf16[128,64]{0,1:T(8,128)(2,1)S(1)}, u32[]{:S(2)}, u32[]{:S(2)}) collective-permute-start(bf16[128,64]{0,1:T(8,128)(2,1)S(1)} %slice.34), channel_id=1, source_target_pairs={{0,8},{8,16},{16,24},{1,9},{9,17},{17,25},{2,10},{10,18},{18,26},{... | collective-permute-start | bytes 49160 | tf_op jit(solution)/shard_map/ppermute | solution.py:18
  22.2 0.8 copy.97
  23.1 1.2 reduce-window.6
  25.9 0.6 fusion.76
  27.0 0.5 fusion.30
  27.7 3.3 %convolution_convert_fusion = bf16[1024,2048]{1,0:T(8,128)(2,1)} fusion(bf16[128,2048]{1,0:T(8,128)(2,1)S(1)} %copy-done, bf16[16,8,8,128]{3,2,1,0:T(8,128)(2,1)S(1)} %bitcast.153), kind=kOutput, calls=%fused_computation.8 | convolution fusion | flops 538968064 | bytes 4980736 | tf_op jit(solution)/shard_map/dot_general | solution.py:87
  31.2 0.8 copy-done.1
  32.3 1.8 convolution_convert_fusion.1
  34.2 4.5 %all-to-all-start = ((bf16[4,1,96,2048]{3,2,1,0:T(8,128)(2,1)}), bf16[4,1,96,2048]{3,2,1,0:T(8,128)(2,1)}, u32[]{:S(2)}, u32[]{:S(2)}) async-start(bf16[4,1,96,2048]{3,2,1,0:T(8,128)(2,1)} %bitcast.13), calls=%async_computation.1 | async-start | bytes 3145728 | tf_op jit(solution)/shard_map/all_to_all | solution.py:120
  39.0 10.4 %collective-permute-done.3 = bf16[1,2048,128]{2,1,0:T(8,128)(2,1)S(1)} collective-permute-done((bf16[1,2048,128]{2,1,0:T(8,128)(2,1)S(1)}, bf16[1,2048,128]{2,1,0:T(8,128)(2,1)S(1)}, u32[]{:S(2)}, u32[]{:S(2)}) %collective-permute-start.3) | collective-permute-done | bytes 524320 | tf_op jit(solution)/shard_map/ppermute | solution.py:126
  49.8 3.5 %collective-permute-start.7 = (bf16[1,2048,128]{2,1,0:T(8,128)(2,1)S(1)}, bf16[1,2048,128]{2,1,0:T(8,128)(2,1)S(1)}, u32[]{:S(2)}, u32[]{:S(2)}) collective-permute-start(bf16[1,2048,128]{2,1,0:T(8,128)(2,1)S(1)} %collective-permute-done.6), channel_id=1, source_target_pairs={{0,7},{1,0},{2,1},{3,2},{4,3},{5,4},{6,5},{7,6},{8,15},{9,8},{10,9... | collective-permute-start | bytes 1572872 | tf_op jit(solution)/shard_map/ppermute | solution.py:128
  53.3 18.6 %collective-permute-done.4 = bf16[1,2048,128]{2,1,0:T(8,128)(2,1)} collective-permute-done((bf16[1,2048,128]{2,1,0:T(8,128)(2,1)S(1)}, bf16[1,2048,128]{2,1,0:T(8,128)(2,1)}, u32[]{:S(2)}, u32[]{:S(2)}) %collective-permute-start.4) | collective-permute-done | bytes 524320 | tf_op jit(solution)/shard_map/ppermute | solution.py:126
  71.9 1.9 collective-permute-start.5
  74.3 3.7 %collective-permute-start.8 = (bf16[1,2048,128]{2,1,0:T(8,128)(2,1)S(1)}, bf16[1,2048,128]{2,1,0:T(8,128)(2,1)S(1)}, u32[]{:S(2)}, u32[]{:S(2)}) collective-permute-start(bf16[1,2048,128]{2,1,0:T(8,128)(2,1)S(1)} %collective-permute-done.7), channel_id=1, source_target_pairs={{0,7},{1,0},{2,1},{3,2},{4,3},{5,4},{6,5},{7,6},{8,15},{9,8},{10,9... | collective-permute-start | bytes 1572872 | tf_op jit(solution)/shard_map/ppermute | solution.py:128
  78.1 4.7 %collective-permute-done.5 = bf16[1,2048,128]{2,1,0:T(8,128)(2,1)} collective-permute-done((bf16[1,2048,128]{2,1,0:T(8,128)(2,1)}, bf16[1,2048,128]{2,1,0:T(8,128)(2,1)}, u32[]{:S(2)}, u32[]{:S(2)}) %collective-permute-start.5) | collective-permute-done | bytes 524320 | tf_op jit(solution)/shard_map/ppermute | solution.py:126
  82.7 2.0 constant_dynamic-update-slice_fusion.15
  84.7 2.0 %constant_dynamic-update-slice_fusion.14 = bf16[1,2048,2048]{2,1,0:T(8,128)(2,1)} fusion(bf16[1,2048,2048]{2,1,0:T(8,128)(2,1)} %constant_dynamic-update-slice_fusion.15, bf16[1,2048,128]{2,1,0:T(8,128)(2,1)} %collective-permute-done.4), kind=kLoop, calls=%fused_computation.86 | loop fusion | bytes 1048576
  86.7 0.9 constant_dynamic-update-slice_fusion.13
  87.6 0.9 constant_dynamic-update-slice_fusion.12
  88.4 0.9 constant_dynamic-update-slice_fusion.11
  89.3 0.9 constant_dynamic-update-slice_fusion.10
  90.2 0.9 constant_dynamic-update-slice_fusion.9
  91.1 0.9 constant_dynamic-update-slice_fusion.8
  92.0 1.9 constant_dynamic-update-slice_fusion.7
  94.0 2.0 constant_dynamic-update-slice_fusion.6
  95.9 0.9 constant_dynamic-update-slice_fusion.5
  96.8 0.9 constant_dynamic-update-slice_fusion.4
  97.7 0.9 constant_dynamic-update-slice_fusion.3
  98.6 0.9 constant_dynamic-update-slice_fusion.2
  99.6 0.9 constant_dynamic-update-slice_fusion.1
  100.4 0.9 constant_dynamic-update-slice_fusion
  101.3 4.6 %fusion.2 = f32[4,96,1024]{2,1,0:T(8,128)S(1)} fusion(bf16[1,2048,1024]{2,1,0:T(8,128)(2,1)} %all-gather.3.cloned.1.call-done, bf16[4,1,96,2048]{3,2,1,0:T(8,128)(2,1)} %all-to-all-done), kind=kOutput, calls=%fused_computation.3 | convolution fusion | flops 1610612736 | bytes 7340032 | tf_op jit(solution)/shard_map/sxcd,xdf->sxcf/dot_general | solution.py:137
  105.9 24.4 %all-gather.5.cloned.1.call-done = bf16[1,2048,1024]{2,1,0:T(8,128)(2,1)} async-done(((bf16[1,2048,128]{2,1,0:T(8,128)(2,1)}), bf16[1,2048,1024]{2,1,0:T(8,128)(2,1)}) %all-gather.5.cloned.1.call-update) | async-done | bytes 4194320 | tf_op jit(solution)/shard_map/all_gather | solution.py:135
  130.3 8.7 %fusion.10 = bf16[4,1,96,2048]{3,2,1,0:T(8,128)(2,1)} fusion(bf16[1,2048,1024]{2,1,0:T(8,128)(2,1)} %all-gather.5.cloned.1.call-done, f32[4,96,1024]{2,1,0:T(8,128)S(1)} %fusion.2, bf16[4,1,96,2048]{3,2,1,0:T(8,128)(2,1)} %all-to-all-done, bf16[1,2048,2048]{2,1,0:T(8,128)(2,1)} %constant_dynamic-update-slice_fusion, s32[]{:T(128)S(6)} %select_n.64), kind=kOutput, calls=%fused_computation.11 | convolution fusion | flops 3224371200 | bytes 13107204 | tf_op jit(solution)/shard_map/sxcf,xdf->sxcd/dot_general | solution.py:139
  138.9 3.8 %all-to-all-start.1 = ((bf16[4,1,96,2048]{3,2,1,0:T(8,128)(2,1)}), bf16[4,1,96,2048]{3,2,1,0:T(8,128)(2,1)S(1)}, u32[]{:S(2)}, u32[]{:S(2)}) async-start(bf16[4,1,96,2048]{3,2,1,0:T(8,128)(2,1)} %fusion.10), calls=%async_computation.2 | async-start | bytes 3145728 | tf_op jit(solution)/shard_map/all_to_all | solution.py:140
  142.9 38.0 %reduce-scatter.2.cloned.1.call-done = bf16[128,2048]{1,0:T(8,128)(2,1)} async-done(((bf16[1024,2048]{1,0:T(8,128)(2,1)}), bf16[128,2048]{1,0:T(8,128)(2,1)}) %reduce-scatter.2.cloned.1.call-update) | async-done | bytes 524304 | tf_op jit(solution)/shard_map/reduce_scatter | solution.py:86
  180.8 1.2 fusion.31
  182.1 2.0 %fusion.33 = bf16[128,2048]{1,0:T(8,128)(2,1)} fusion(bf16[128,2048]{1,0:T(8,128)(2,1)} %reduce-scatter.2.cloned.1.call-done, f32[2048]{0:T(1024)S(1)} %copy-done.6, f32[128]{0:T(128)S(1)} %add_rsqrt_fusion.2), kind=kLoop, calls=%fused_computation.37 | loop fusion | flops 1048576 | bytes 1057280 | tf_op jit(solution)/shard_map/convert_element_type | solution.py:92
  184.1 1.4 gather_fusion
  185.5 0.7 gather.7
  186.2 4.1 %multiply_reduce_fusion = f32[128,2048]{1,0:T(8,128)S(1)} fusion(bf16[128,2,2048]{2,1,0:T(2,128)(2,1)S(1)} %gather.7, pred[128,2]{1,0:T(8,128)(4,1)S(1)} %copy.102, f32[128,2]{1,0:T(8,128)S(1)} %copy.96), kind=kLoop, calls=%fused_computation.14 | loop fusion | flops 1835008 | bytes 2098432 | tf_op jit(solution)/shard_map/reduce_sum | solution.py:147
  190.5 1.0 multiply_convert_fusion
  (92 shorter events, 4.8 us)
Async XLA Ops:
  7.2 20.5 %copy-start = (bf16[128,2048]{1,0:T(8,128)(2,1)S(1)}, bf16[128,2048]{1,0:T(8,128)(2,1)}, u32[]{:S(2)}) copy-start(bf16[128,2048]{1,0:T(8,128)(2,1)} %param.21) | copy-start | bytes 1572868
  7.2 18.1 %copy-start.9 = (f32[2]{0:T(128)S(1)}, f32[2]{0:T(128)}, u32[]{:S(2)}) copy-start(f32[2]{0:T(128)} %param.19) | copy-start | bytes 28
  7.2 18.4 %copy-start.3 = (bf16[1024,128]{1,0:T(8,128)(2,1)S(1)}, bf16[1024,128]{1,0:T(8,128)(2,1)}, u32[]{:S(2)}) copy-start(bf16[1024,128]{1,0:T(8,128)(2,1)} %param.16) | copy-start | bytes 786436
  7.2 94.1 %all-gather.3.cloned.1.call-start = ((), (), s32[]{:S(2)}) async-start(), calls=%async_computation.4 | async-start | bytes 4718592 | tf_op jit(solution)/shard_map/all_gather | solution.py:134
  7.9 122.3 %all-gather.5.cloned.1.call-start = ((), (), s32[]{:S(2)}) async-start(), calls=%async_computation.5 | async-start | bytes 4718592 | tf_op jit(solution)/shard_map/all_gather | solution.py:135
  8.7 172.1 %reduce-scatter.2.cloned.1.call-start = ((), (), s32[]{:S(2)}) async-start(), calls=%async_computation.3 | async-start | bytes 4718592 | tf_op jit(solution)/shard_map/reduce_scatter | solution.py:86
  8.7 23.5 %collective-permute-start.2 = (bf16[1,2048,128]{2,1,0:T(8,128)(2,1)}, bf16[1,2048,128]{2,1,0:T(8,128)(2,1)S(1)}, u32[]{:S(2)}, u32[]{:S(2)}) collective-permute-start(bf16[1,2048,128]{2,1,0:T(8,128)(2,1)} %param.29), channel_id=1, source_target_pairs={{0,1},{1,2},{2,3},{3,4},{4,5},{5,6},{6,7},{7,0},{8,9},{9,10},{10,1... | collective-permute-start | bytes 1572872 | tf_op jit(solution)/shard_map/ppermute | solution.py:126
  9.3 40.5 %collective-permute-start.6 = (bf16[1,2048,128]{2,1,0:T(8,128)(2,1)}, bf16[1,2048,128]{2,1,0:T(8,128)(2,1)S(1)}, u32[]{:S(2)}, u32[]{:S(2)}) collective-permute-start(bf16[1,2048,128]{2,1,0:T(8,128)(2,1)} %param.29), channel_id=1, source_target_pairs={{0,7},{1,0},{2,1},{3,2},{4,3},{5,4},{6,5},{7,6},{8,15},{9,8},{10,9... | collective-permute-start | bytes 1572872 | tf_op jit(solution)/shard_map/ppermute | solution.py:128
  14.6 11.9 %copy-start.8 = (f32[2]{0:T(128)S(1)}, f32[2]{0:T(128)}, u32[]{:S(2)}) copy-start(f32[2]{0:T(128)} %param.20) | copy-start | bytes 28
  14.8 11.1 %collective-permute-start.1 = (bf16[128,64]{0,1:T(8,128)(2,1)S(1)}, bf16[128,64]{0,1:T(8,128)(2,1)S(1)}, u32[]{:S(2)}, u32[]{:S(2)}) collective-permute-start(bf16[128,64]{0,1:T(8,128)(2,1)S(1)} %slice.36), channel_id=1, source_target_pairs={{0,8},{8,16},{16,24},{1,9},{9,17},{17,25},{2,10},{10,18},{18,26},{... | collective-permute-start | bytes 49160 | tf_op jit(solution)/shard_map/ppermute | solution.py:18
  18.8 8.2 %collective-permute-start = (bf16[128,64]{0,1:T(8,128)(2,1)S(1)}, bf16[128,64]{0,1:T(8,128)(2,1)S(1)}, u32[]{:S(2)}, u32[]{:S(2)}) collective-permute-start(bf16[128,64]{0,1:T(8,128)(2,1)S(1)} %slice.34), channel_id=1, source_target_pairs={{0,8},{8,16},{16,24},{1,9},{9,17},{17,25},{2,10},{10,18},{18,26},{... | collective-permute-start | bytes 49160 | tf_op jit(solution)/shard_map/ppermute | solution.py:18
  30.9 1.0 copy-start.1
  30.9 1.2 copy-start.4
  30.9 1.4 copy-start.5
  30.9 7.7 %copy-start.10 = (bf16[2048,4]{0,1:T(4,128)(2,1)S(1)}, bf16[2048,4]{0,1:T(4,128)(2,1)}, u32[]{:S(2)}) copy-start(bf16[2048,4]{0,1:T(4,128)(2,1)} %param.26) | copy-start | bytes 49156
  31.0 18.5 %copy-start.11 = (bf16[2048,4]{0,1:T(4,128)(2,1)S(1)}, bf16[2048,4]{0,1:T(4,128)(2,1)}, u32[]{:S(2)}) copy-start(bf16[2048,4]{0,1:T(4,128)(2,1)} %param.27) | copy-start | bytes 49156
  32.2 17.2 %collective-permute-start.3 = (bf16[1,2048,128]{2,1,0:T(8,128)(2,1)S(1)}, bf16[1,2048,128]{2,1,0:T(8,128)(2,1)S(1)}, u32[]{:S(2)}, u32[]{:S(2)}) collective-permute-start(bf16[1,2048,128]{2,1,0:T(8,128)(2,1)S(1)} %collective-permute-done.2), channel_id=1, source_target_pairs={{0,1},{1,2},{2,3},{3,4},{4,5},{5,6},{6,7},{7,0},{8,9},{9,10},{10,1... | collective-permute-start | bytes 1572872 | tf_op jit(solution)/shard_map/ppermute | solution.py:126
  34.2 54.3 %copy-start.2 = (bf16[1,2048,128]{2,1,0:T(8,128)(2,1)S(1)}, bf16[1,2048,128]{2,1,0:T(8,128)(2,1)}, u32[]{:S(2)}) copy-start(bf16[1,2048,128]{2,1,0:T(8,128)(2,1)} %param.29) | copy-start | bytes 1572868
  34.2 67.1 %all-to-all-start = ((bf16[4,1,96,2048]{3,2,1,0:T(8,128)(2,1)}), bf16[4,1,96,2048]{3,2,1,0:T(8,128)(2,1)}, u32[]{:S(2)}, u32[]{:S(2)}) async-start(bf16[4,1,96,2048]{3,2,1,0:T(8,128)(2,1)} %bitcast.13), calls=%async_computation.1 | async-start | bytes 3145728 | tf_op jit(solution)/shard_map/all_to_all | solution.py:120
  49.4 22.5 %collective-permute-start.4 = (bf16[1,2048,128]{2,1,0:T(8,128)(2,1)S(1)}, bf16[1,2048,128]{2,1,0:T(8,128)(2,1)}, u32[]{:S(2)}, u32[]{:S(2)}) collective-permute-start(bf16[1,2048,128]{2,1,0:T(8,128)(2,1)S(1)} %collective-permute-done.3), channel_id=1, source_target_pairs={{0,1},{1,2},{2,3},{3,4},{4,5},{5,6},{6,7},{7,0},{8,9},{9,10},{10,1... | collective-permute-start | bytes 1572872 | tf_op jit(solution)/shard_map/ppermute | solution.py:126
  49.8 24.6 %collective-permute-start.7 = (bf16[1,2048,128]{2,1,0:T(8,128)(2,1)S(1)}, bf16[1,2048,128]{2,1,0:T(8,128)(2,1)S(1)}, u32[]{:S(2)}, u32[]{:S(2)}) collective-permute-start(bf16[1,2048,128]{2,1,0:T(8,128)(2,1)S(1)} %collective-permute-done.6), channel_id=1, source_target_pairs={{0,7},{1,0},{2,1},{3,2},{4,3},{5,4},{6,5},{7,6},{8,15},{9,8},{10,9... | collective-permute-start | bytes 1572872 | tf_op jit(solution)/shard_map/ppermute | solution.py:128
  71.9 10.8 %collective-permute-start.5 = (bf16[1,2048,128]{2,1,0:T(8,128)(2,1)}, bf16[1,2048,128]{2,1,0:T(8,128)(2,1)}, u32[]{:S(2)}, u32[]{:S(2)}) collective-permute-start(bf16[1,2048,128]{2,1,0:T(8,128)(2,1)} %collective-permute-done.4), channel_id=1, source_target_pairs={{0,1},{1,2},{2,3},{3,4},{4,5},{5,6},{6,7},{7,0},{8,9},{9,10},{10,1... | collective-permute-start | bytes 1572872 | tf_op jit(solution)/shard_map/ppermute | solution.py:126
  74.3 16.8 %collective-permute-start.8 = (bf16[1,2048,128]{2,1,0:T(8,128)(2,1)S(1)}, bf16[1,2048,128]{2,1,0:T(8,128)(2,1)S(1)}, u32[]{:S(2)}, u32[]{:S(2)}) collective-permute-start(bf16[1,2048,128]{2,1,0:T(8,128)(2,1)S(1)} %collective-permute-done.7), channel_id=1, source_target_pairs={{0,7},{1,0},{2,1},{3,2},{4,3},{5,4},{6,5},{7,6},{8,15},{9,8},{10,9... | collective-permute-start | bytes 1572872 | tf_op jit(solution)/shard_map/ppermute | solution.py:128
  105.9 76.2 %copy-start.6 = (f32[2048]{0:T(1024)S(1)}, f32[2048]{0:T(1024)}, u32[]{:S(2)}) copy-start(f32[2048]{0:T(1024)} %param.22) | copy-start | bytes 24580
  138.9 45.2 %all-to-all-start.1 = ((bf16[4,1,96,2048]{3,2,1,0:T(8,128)(2,1)}), bf16[4,1,96,2048]{3,2,1,0:T(8,128)(2,1)S(1)}, u32[]{:S(2)}, u32[]{:S(2)}) async-start(bf16[4,1,96,2048]{3,2,1,0:T(8,128)(2,1)} %fusion.10), calls=%async_computation.2 | async-start | bytes 3145728 | tf_op jit(solution)/shard_map/all_to_all | solution.py:140
  185.5 5.0 %copy-start.7 = (f32[2048]{0:T(1024)S(1)}, f32[2048]{0:T(1024)}, u32[]{:S(2)}) copy-start(f32[2048]{0:T(1024)} %param.25) | copy-start | bytes 24580
Sparse Core Ops, SparseCore 0:
  9.6 65.6 all-gather.2
  76.8 53.3 all-gather.4
  132.6 48.2 reduce-scatter.1
